TPU v7x, 32 devices: a whole 2x2x4 slice. The times are simulated.
32 devices in a mesh: gr: 2 (over x), fs: 8 (over z, y), tp: 2 (over core).
Axes of the slice: x: 2, y: 2, z: 4, core: 2. Of those that a mesh axis runs over, the one named last changes fastest.
Arguments:
- tokens: bfloat16 [4, 2048, 2048], P(('gr', 'tp')), may hold values from -6 to 6
- gate_master: float32 [3, 2048, 7168], P(None, 'fs', ('gr', 'tp')), may hold values from -0.125 to 0.125
- up_master: float32 [3, 2048, 7168], P(None, 'fs', ('gr', 'tp')), may hold values from -0.125 to 0.125
- down_master: float32 [3, 7168, 2048], P(None, 'fs', ('gr', 'tp')), may hold values from -0.0625 to 0.0625
- norm_gain: float32 [2048], P('fs'), may hold values from 0.1 to 1.9
- route: int32 [4, 2048, 2], P(('gr', 'tp')), may hold values from 0 to 2, all different within a row
- route_weight: float32 [4, 2048, 2], P(('gr', 'tp')), may hold values from 0.05 to 1
Outputs:
- gate_out: bfloat16 [3, 2048, 7168], P(None, None, 'fs')
- up_out: bfloat16 [3, 2048, 7168], P(None, None, 'fs')
- down_out: bfloat16 [3, 7168, 2048], P(None, 'fs')
- mixed: bfloat16 [4, 2048, 2048], P(('gr', 'tp'), 'fs')
Inputs may be any that keep to these rules, and one draw needn't show every extreme that they name: `route`: each token names two different experts; every expert is named by some token.
All inputs are finite; a program needn't handle non-finite values.
Results may differ from a plain program's by a relative error of at most 0.024.
Values may be sent and summed in bfloat16 or wider, within the bound.
A program may use at most 192 MiB of HBM per device.

v0:
```python
import jax
import jax.numpy as jnp
from jax import lax
from jax.sharding import PartitionSpec as P


def normalize(rows_in):
    values = rows_in.astype(jnp.float32)
    scaled = values * lax.rsqrt(jnp.mean(values * values, axis=-1, keepdims=True) + 1e-06)
    return scaled.astype(jnp.bfloat16)


def mixing(chosen, weights, experts):
    share = weights / jnp.sum(weights, axis=-1, keepdims=True)
    labels = jnp.arange(experts, dtype=jnp.int32)
    match = (chosen[:, :, None] == labels[None, None, :]).astype(jnp.float32)
    return jnp.sum(share[:, :, None] * match, axis=1)


def expert_term(normed, mix_column, gate_weight, up_weight, down_weight):
    gate_act = jnp.dot(normed, gate_weight, preferred_element_type=jnp.float32)
    up_act = jnp.dot(normed, up_weight, preferred_element_type=jnp.float32)
    hidden = (jax.nn.silu(gate_act) * up_act).astype(jnp.bfloat16)
    projected = jnp.dot(hidden, down_weight, preferred_element_type=jnp.float32)
    return mix_column * projected


def shards(tokens, gate_master, up_master, down_master, norm_gain, route, route_weight):
    scaled_gain = norm_gain[None, :, None]
    gate_local = (scaled_gain * gate_master).astype(jnp.bfloat16)
    up_local = (scaled_gain * up_master).astype(jnp.bfloat16)
    down_local = down_master.astype(jnp.bfloat16)
    experts = gate_local.shape[0]
    normed = normalize(tokens[0])
    combine = mixing(route[0], route_weight[0], experts)
    width = normed.shape[1]
    gate_list = []
    up_list = []
    down_list = []
    total = jnp.zeros((normed.shape[0], width), jnp.float32)
    for index in range(experts):
        gate_rows, up_rows, down_full = (
            lax.all_gather(gate_local[index], ("gr", "tp"), axis=1, tiled=True),
            lax.all_gather(up_local[index], ("gr", "tp"), axis=1, tiled=True),
            lax.all_gather(down_local[index], ("gr", "tp"), axis=1, tiled=True),
        )
        gate_block, up_block = (
            lax.all_to_all(gate_rows, "fs", split_axis=1, concat_axis=0, tiled=True),
            lax.all_to_all(up_rows, "fs", split_axis=1, concat_axis=0, tiled=True),
        )
        total = total + expert_term(
            normed, combine[:, index : index + 1], gate_block, up_block, down_full
        )
        gate_list.append(gate_block)
        up_list.append(up_block)
        down_list.append(down_full)
    gate_out = jnp.stack(gate_list, axis=0)
    up_out = jnp.stack(up_list, axis=0)
    down_out = jnp.stack(down_list, axis=0)
    summed = lax.psum_scatter(total.astype(jnp.bfloat16), "fs", scatter_dimension=0, tiled=True)
    mixed = summed[None]
    return (gate_out, up_out, down_out, mixed)


def solution(mesh):
    in_specs = (
        P(("gr", "tp"), None, None),
        P(None, "fs", ("gr", "tp")),
        P(None, "fs", ("gr", "tp")),
        P(None, "fs", ("gr", "tp")),
        P("fs"),
        P(("gr", "tp"), None, None),
        P(("gr", "tp"), None, None),
    )
    out_specs = (
        P(None, None, "fs"),
        P(None, None, "fs"),
        P(None, "fs", None),
        P(("gr", "tp"), "fs", None),
    )
    return jax.shard_map(shards, mesh=mesh, in_specs=in_specs, out_specs=out_specs, check_vma=False)
```

profile of v0, /device:TPU:0, one launch (start us, length us, event | category | flops | bytes accessed | tf_op | source)
XLA Modules:
  0.0 764.3 jit_solution(10125969847166633548)
XLA Ops:
  7.2 5.2 multiply_convert_fusion.3
  12.4 1.6 fusion.29
  14.1 1.6 fusion.28
  15.7 0.7 all-gather.19.cloned.1.call-update
  16.5 0.5 all-gather.25.cloned.1.call-update
  17.0 31.4 %all-gather.21.cloned.1.call-done = bf16[1,256,7168]{2,1,0:T(8,128)(2,1)} async-done(((bf16[1,256,1792]{2,1,0:T(8,128)(2,1)}), bf16[1,256,7168]{2,1,0:T(8,128)(2,1)}) %all-gather.21.cloned.1.call-update) | async-done | bytes 3670032 | tf_op jit(solution)/shard_map/all_gather | solution.py:43
  48.4 2.8 copy.34
  51.2 2.4 copy.28
  53.6 5.5 all-to-all-start.1
  59.2 0.5 all-gather.23.cloned.1.call-update
  59.7 22.3 %all-gather.27.cloned.1.call-done = bf16[1,256,7168]{2,1,0:T(8,128)(2,1)} async-done(((bf16[1,256,1792]{2,1,0:T(8,128)(2,1)}), bf16[1,256,7168]{2,1,0:T(8,128)(2,1)}) %all-gather.27.cloned.1.call-update) | async-done | bytes 3670032 | tf_op jit(solution)/shard_map/all_gather | solution.py:44
  82.0 2.8 copy.37
  84.8 2.4 copy.31
  87.3 54.3 %all-to-all-done.1 = bf16[256,8,896]{2,0,1:T(8,128)(2,1)} async-done(((bf16[256,8,896]{2,0,1:T(8,128)(2,1)}), bf16[256,8,896]{2,0,1:T(8,128)(2,1)}, u32[]{:S(2)}, u32[]{:S(2)}) %all-to-all-start.1) | async-done | bytes 3670048 | tf_op jit(solution)/shard_map/all_to_all | solution.py:48
  141.6 4.5 all-to-all-start.4
  146.2 0.5 all-gather.29.cloned.1.call-update
  146.7 2.8 copy.33
  149.5 2.4 copy.27
  151.9 75.7 %all-to-all-done.4 = bf16[256,8,896]{2,0,1:T(8,128)(2,1)} async-done(((bf16[256,8,896]{2,0,1:T(8,128)(2,1)}), bf16[256,8,896]{2,0,1:T(8,128)(2,1)}, u32[]{:S(2)}, u32[]{:S(2)}) %all-to-all-start.4) | async-done | bytes 3670048 | tf_op jit(solution)/shard_map/all_to_all | solution.py:49
  227.6 4.5 all-to-all-start
  232.2 2.9 convert_element_type.45
  235.1 1.6 fusion.27
  236.8 0.7 all-gather.31.cloned.1.call-update
  237.5 2.8 copy.36
  240.3 2.4 copy.30
  242.7 70.7 %all-to-all-done = bf16[256,8,896]{2,0,1:T(8,128)(2,1)} async-done(((bf16[256,8,896]{2,0,1:T(8,128)(2,1)}), bf16[256,8,896]{2,0,1:T(8,128)(2,1)}, u32[]{:S(2)}, u32[]{:S(2)}) %all-to-all-start) | async-done | bytes 3670048 | tf_op jit(solution)/shard_map/all_to_all | solution.py:48
  313.5 4.5 all-to-all-start.3
  318.0 0.7 all-gather.35.cloned.1.call-update
  318.9 5.1 fusion
  324.0 2.8 copy.35
  326.8 2.4 copy.29
  329.2 70.1 %all-to-all-done.3 = bf16[256,8,896]{2,0,1:T(8,128)(2,1)} async-done(((bf16[256,8,896]{2,0,1:T(8,128)(2,1)}), bf16[256,8,896]{2,0,1:T(8,128)(2,1)}, u32[]{:S(2)}, u32[]{:S(2)}) %all-to-all-start.3) | async-done | bytes 3670048 | tf_op jit(solution)/shard_map/all_to_all | solution.py:49
  399.3 16.6 %all-to-all-start.2 = ((bf16[256,8,896]{2,0,1:T(8,128)(2,1)}), bf16[256,8,896]{2,0,1:T(8,128)(2,1)}, u32[]{:S(2)}, u32[]{:S(2)}) async-start(bf16[256,8,896]{2,0,1:T(8,128)(2,1)} %copy.29), calls=%async_computation.2 | async-start | bytes 7340032 | tf_op jit(solution)/shard_map/all_to_all | solution.py:48
  416.0 2.8 copy.38
  418.8 2.4 copy.32
  421.2 14.2 %fusion.21 = f32[2048,896]{1,0:T(8,128)} fusion(bf16[2048,896]{1,0:T(8,128)(2,1)} %bitcast.20, bf16[1,2048,2048]{2,1,0:T(8,128)(2,1)} %param.7, f32[2048]{0:T(1024)S(1)} %add_rsqrt_fusion), kind=kOutput, calls=%fused_computation.30 | convolution fusion | flops 7528775680 | bytes 19406848 | tf_op jit(solution)/shard_map/dot_general | solution.py:21
  435.5 26.7 %fusion.3 = f32[2048,2048]{1,0:T(8,128)} fusion(f32[2048,896]{1,0:T(8,128)} %fusion.21, bf16[2048,896]{1,0:T(8,128)(2,1)} %bitcast.21, bf16[1,896,2048]{2,1,0:T(8,128)(2,1)} %all-gather.33.cloned.1.call-done, bf16[1,2048,2048]{2,1,0:T(8,128)(2,1)} %param.7, f32[2048]{0:T(1024)S(1)} %add_rsqrt_fusion), kind=kOutput, calls=%fused_computation.14 | convolution fusion | flops 15055978496 | bytes 39854080 | tf_op jit(solution)/shard_map/dot_general | solution.py:24
  462.2 35.0 %all-to-all-done.2 = bf16[256,8,896]{2,0,1:T(8,128)(2,1)} async-done(((bf16[256,8,896]{2,0,1:T(8,128)(2,1)}), bf16[256,8,896]{2,0,1:T(8,128)(2,1)}, u32[]{:S(2)}, u32[]{:S(2)}) %all-to-all-start.2) | async-done | bytes 3670048 | tf_op jit(solution)/shard_map/all_to_all | solution.py:48
  497.2 4.5 all-to-all-start.5
  501.8 14.2 %fusion.25 = f32[2048,896]{1,0:T(8,128)} fusion(bf16[2048,896]{1,0:T(8,128)(2,1)} %bitcast.16, bf16[1,2048,2048]{2,1,0:T(8,128)(2,1)} %param.7, f32[2048]{0:T(1024)S(1)} %add_rsqrt_fusion), kind=kOutput, calls=%fused_computation.31 | convolution fusion | flops 7528775680 | bytes 19406848 | tf_op jit(solution)/shard_map/dot_general | solution.py:21
  516.0 14.2 %fusion.17 = f32[2048,896]{1,0:T(8,128)} fusion(bf16[2048,896]{1,0:T(8,128)(2,1)} %bitcast.24, bf16[1,2048,2048]{2,1,0:T(8,128)(2,1)} %param.7, f32[2048]{0:T(1024)S(1)} %add_rsqrt_fusion), kind=kOutput, calls=%fused_computation.29 | convolution fusion | flops 7528775680 | bytes 19406848 | tf_op jit(solution)/shard_map/dot_general | solution.py:21
  530.2 26.9 %fusion.4 = f32[2048,2048]{1,0:T(8,128)} fusion(f32[2048,896]{1,0:T(8,128)} %fusion.25, bf16[2048,896]{1,0:T(8,128)(2,1)} %bitcast.17, bf16[1,896,2048]{2,1,0:T(8,128)(2,1)} %all-gather.31.cloned.1.call-done, bf16[1,2048,2048]{2,1,0:T(8,128)(2,1)} %param.7, f32[2048]{0:T(1024)S(1)} %add_rsqrt_fusion), kind=kOutput, calls=%fused_computation.15 | convolution fusion | flops 15055978496 | bytes 39854080 | tf_op jit(solution)/shard_map/dot_general | solution.py:24
  557.1 25.8 %all-to-all-done.5 = bf16[256,8,896]{2,0,1:T(8,128)(2,1)} async-done(((bf16[256,8,896]{2,0,1:T(8,128)(2,1)}), bf16[256,8,896]{2,0,1:T(8,128)(2,1)}, u32[]{:S(2)}, u32[]{:S(2)}) %all-to-all-start.5) | async-done | bytes 3670048 | tf_op jit(solution)/shard_map/all_to_all | solution.py:49
  582.9 28.4 %add_convert_fusion = bf16[2048,2048]{1,0:T(8,128)(2,1)} fusion(f32[2048,2048]{1,0:T(8,128)} %fusion.3, f32[2048,2048]{1,0:T(8,128)} %fusion.4, f32[2048]{0:T(1024)S(1)} %bitcast.95, f32[2048]{0:T(1024)S(1)} %bitcast.96, f32[2048]{0:T(1024)S(1)} %bitcast.94, f32[2048,896]{1,0:T(8,128)} %fusion.17, bf16[2048,896]{1,0:T(8,128)(2,1)} %bitcast.25, ...), kind=kOutput, calls=%fused_computation.4 | convolution fusion | flops 15081144320 | bytes 65044480 | tf_op jit(solution)/shard_map/dot_general | solution.py:24
  611.3 9.8 %pad_maximum_fusion.2 = bf16[3,896,2048]{2,1,0:T(8,128)(2,1)} fusion(bf16[1,896,2048]{2,1,0:T(8,128)(2,1)} %all-gather.35.cloned.1.call-done, bf16[1,896,2048]{2,1,0:T(8,128)(2,1)} %all-gather.33.cloned.1.call-done, bf16[1,896,2048]{2,1,0:T(8,128)(2,1)} %all-gather.31.cloned.1.call-done), kind=kLoop, calls=%fused_computation.7 | loop fusion | flops 11010048 | bytes 22020096 | tf_op jit(solution)/shard_map/stack | solution.py:59
  621.1 9.8 %pad_maximum_fusion.1 = bf16[3,2048,896]{2,1,0:T(8,128)(2,1)} fusion(bf16[1,2048,896]{2,1,0:T(8,128)(2,1)} %bitcast.11, bf16[1,2048,896]{2,1,0:T(8,128)(2,1)} %bitcast.9, bf16[1,2048,896]{2,1,0:T(8,128)(2,1)} %bitcast.7), kind=kLoop, calls=%fused_computation.6 | loop fusion | flops 11010048 | bytes 22020096 | tf_op jit(solution)/shard_map/stack | solution.py:58
  630.9 9.8 %pad_maximum_fusion = bf16[3,2048,896]{2,1,0:T(8,128)(2,1)} fusion(bf16[1,2048,896]{2,1,0:T(8,128)(2,1)} %bitcast.5, bf16[1,2048,896]{2,1,0:T(8,128)(2,1)} %bitcast.3, bf16[1,2048,896]{2,1,0:T(8,128)(2,1)} %bitcast.1), kind=kLoop, calls=%fused_computation.5 | loop fusion | flops 11010048 | bytes 22020096 | tf_op jit(solution)/shard_map/stack | solution.py:57
  640.6 116.5 %reduce-scatter.2.cloned.1.call-done = bf16[256,2048]{1,0:T(8,128)(2,1)} async-done(((bf16[2048,2048]{1,0:T(8,128)(2,1)}), bf16[256,2048]{1,0:T(8,128)(2,1)}) %reduce-scatter.2.cloned.1.call-update) | async-done | bytes 1048592 | tf_op jit(solution)/shard_map/reduce_scatter | solution.py:60
  (30 shorter events, 0.7 us)
Async XLA Ops:
  7.2 41.2 %all-gather.21.cloned.1.call-start = ((), (), s32[]{:S(2)}) async-start(), calls=%async_computation.9 | async-start | bytes 4587520 | tf_op jit(solution)/shard_map/all_gather | solution.py:43
  14.0 68.0 %all-gather.27.cloned.1.call-start = ((), (), s32[]{:S(2)}) async-start(), calls=%async_computation.12 | async-start | bytes 4587520 | tf_op jit(solution)/shard_map/all_gather | solution.py:44
  15.7 131.0 %all-gather.19.cloned.1.call-start = ((), (), s32[]{:S(2)}) async-start(), calls=%async_computation.8 | async-start | bytes 4587520 | tf_op jit(solution)/shard_map/all_gather | solution.py:43
  16.4 221.1 %all-gather.25.cloned.1.call-start = ((), (), s32[]{:S(2)}) async-start(), calls=%async_computation.11 | async-start | bytes 4587520 | tf_op jit(solution)/shard_map/all_gather | solution.py:44
  53.6 88.0 %all-to-all-start.1 = ((bf16[256,8,896]{2,0,1:T(8,128)(2,1)}), bf16[256,8,896]{2,0,1:T(8,128)(2,1)}, u32[]{:S(2)}, u32[]{:S(2)}) async-start(bf16[256,8,896]{2,0,1:T(8,128)(2,1)} %copy.28), calls=%async_computation.1 | async-start | bytes 7340032 | tf_op jit(solution)/shard_map/all_to_all | solution.py:48
  59.1 264.9 %all-gather.23.cloned.1.call-start = ((), (), s32[]{:S(2)}) async-start(), calls=%async_computation.10 | async-start | bytes 4587520 | tf_op jit(solution)/shard_map/all_gather | solution.py:43
  141.6 86.0 %all-to-all-start.4 = ((bf16[256,8,896]{2,0,1:T(8,128)(2,1)}), bf16[256,8,896]{2,0,1:T(8,128)(2,1)}, u32[]{:S(2)}, u32[]{:S(2)}) async-start(bf16[256,8,896]{2,0,1:T(8,128)(2,1)} %copy.31), calls=%async_computation.4 | async-start | bytes 7340032 | tf_op jit(solution)/shard_map/all_to_all | solution.py:49
  146.1 269.9 %all-gather.29.cloned.1.call-start = ((), (), s32[]{:S(2)}) async-start(), calls=%async_computation.13 | async-start | bytes 4587520 | tf_op jit(solution)/shard_map/all_gather | solution.py:44
  227.6 85.9 %all-to-all-start = ((bf16[256,8,896]{2,0,1:T(8,128)(2,1)}), bf16[256,8,896]{2,0,1:T(8,128)(2,1)}, u32[]{:S(2)}, u32[]{:S(2)}) async-start(bf16[256,8,896]{2,0,1:T(8,128)(2,1)} %copy.27), calls=%async_computation | async-start | bytes 7340032 | tf_op jit(solution)/shard_map/all_to_all | solution.py:48
  232.1 203.3 %all-gather.33.cloned.1.call-start = ((), (), s32[]{:S(2)}) async-start(), calls=%async_computation.15 | async-start | bytes 4587520 | tf_op jit(solution)/shard_map/all_gather | solution.py:45
  236.7 293.5 %all-gather.31.cloned.1.call-start = ((), (), s32[]{:S(2)}) async-start(), calls=%async_computation.14 | async-start | bytes 4587520 | tf_op jit(solution)/shard_map/all_gather | solution.py:45
  240.3 78.5 %copy-start = (f32[1,2048,2]{1,2,0:T(2,128)S(1)}, f32[1,2048,2]{1,2,0:T(2,128)}, u32[]{:S(2)}) copy-start(f32[1,2048,2]{1,2,0:T(2,128)} %param.13) | copy-start | bytes 49156
  240.3 78.5 %copy-start.1 = (s32[1,2048,2]{1,2,0:T(2,128)S(1)}, s32[1,2048,2]{1,2,0:T(2,128)}, u32[]{:S(2)}) copy-start(s32[1,2048,2]{1,2,0:T(2,128)} %param.12) | copy-start | bytes 49156
  313.5 85.9 %all-to-all-start.3 = ((bf16[256,8,896]{2,0,1:T(8,128)(2,1)}), bf16[256,8,896]{2,0,1:T(8,128)(2,1)}, u32[]{:S(2)}, u32[]{:S(2)}) async-start(bf16[256,8,896]{2,0,1:T(8,128)(2,1)} %copy.30), calls=%async_computation.3 | async-start | bytes 7340032 | tf_op jit(solution)/shard_map/all_to_all | solution.py:49
  318.0 239.1 %all-gather.35.cloned.1.call-start = ((), (), s32[]{:S(2)}) async-start(), calls=%async_computation.16 | async-start | bytes 4587520 | tf_op jit(solution)/shard_map/all_gather | solution.py:45
  399.3 97.9 %all-to-all-start.2 = ((bf16[256,8,896]{2,0,1:T(8,128)(2,1)}), bf16[256,8,896]{2,0,1:T(8,128)(2,1)}, u32[]{:S(2)}, u32[]{:S(2)}) async-start(bf16[256,8,896]{2,0,1:T(8,128)(2,1)} %copy.29), calls=%async_computation.2 | async-start | bytes 7340032 | tf_op jit(solution)/shard_map/all_to_all | solution.py:48
  497.2 85.7 %all-to-all-start.5 = ((bf16[256,8,896]{2,0,1:T(8,128)(2,1)}), bf16[256,8,896]{2,0,1:T(8,128)(2,1)}, u32[]{:S(2)}, u32[]{:S(2)}) async-start(bf16[256,8,896]{2,0,1:T(8,128)(2,1)} %copy.32), calls=%async_computation.5 | async-start | bytes 7340032 | tf_op jit(solution)/shard_map/all_to_all | solution.py:49
  501.7 255.4 %reduce-scatter.2.cloned.1.call-start = ((), (), s32[]{:S(2)}) async-start(), calls=%async_computation.7 | async-start | bytes 9437184 | tf_op jit(solution)/shard_map/reduce_scatter | solution.py:60
Sparse Core Ops, SparseCore 0:
  14.1 34.1 all-gather.20
  50.5 31.4 all-gather.26
  84.2 31.4 all-gather.18
  117.7 31.4 all-gather.24
  150.6 31.4 all-gather.22
  183.5 31.4 all-gather.28
  236.8 31.8 all-gather.32
  270.8 31.4 all-gather.30
  320.4 31.8 all-gather.34
  611.5 145.5 reduce-scatter.1
where the time goes:
time: 773 us; the launch traced here: 764 us
  waiting for transfers between devices  506 us (65%)
  matrix products  125 us (16%)
  other arithmetic  42.6 us (6%)
  starting transfers between devices  40.6 us (5%)
  local copies, waits for them, and re-layouts  36.1 us (5%)
  between operations  14.8 us (2%)
    all_to_all x3, waiting for transfers between devices, shards(): lax.all_to_all(up_rows, 'fs', split_axis=1, concat_axis=0, tiled=True)  172 us
    all_to_all x3, waiting for transfers between devices, shards(): lax.all_to_all(gate_rows, 'fs', split_axis=1, concat_axis=0, tiled=True)  160 us
    reduce_scatter x1, waiting for transfers between devices, shards(): lax.psum_scatter(total.astype(jnp.bfloat16), 'fs', scatter_dimension=0, t...  116 us
    dot_general x3, matrix products, expert_term(): projected = jnp.dot(hidden, down_weight, preferred_element_type=jnp.float32)  82 us
    dot_general x3, matrix products, expert_term(): gate_act = jnp.dot(normed, gate_weight, preferred_element_type=jnp.float32)  42.7 us
    all_gather x3, waiting for transfers between devices, shards(): lax.all_gather(gate_local[index], ('gr', 'tp'), axis=1, tiled=True)  31.4 us
    all_to_all x3, starting transfers between devices, shards(): lax.all_to_all(gate_rows, 'fs', split_axis=1, concat_axis=0, tiled=True)  26.6 us
    all_gather x3, waiting for transfers between devices, shards(): lax.all_gather(up_local[index], ('gr', 'tp'), axis=1, tiled=True)  22.4 us
  transfers between devices with their start and end apart: 16, of which 9 were waited for; matrix products, arithmetic and copies ran while one was open for 22% of the time, Pallas kernels for 0%

commit v1 on v0

--- a/solution.py
+++ b/solution.py
@@ -2,6 +2,29 @@
 import jax.numpy as jnp
 from jax import lax
 from jax.sharding import PartitionSpec as P
+
+
+def split_up(shard, dim, devices):
+    dims = shard.shape
+    tiles = shard.reshape(*dims[:dim], devices, dims[dim] // devices, *dims[dim + 1 :])
+    return jnp.moveaxis(tiles, dim, 0)
+
+
+def joined_along(pieces, dim):
+    pieces = jnp.moveaxis(pieces, 0, dim)
+    shape = pieces.shape
+    return pieces.reshape(*shape[:dim], shape[dim] * shape[dim + 1], *shape[dim + 2 :])
+
+
+def swapped_with_each(x, axis, split_dim, concat_dim):
+    size, index = (lax.axis_size(axis), lax.axis_index(axis))
+    pieces = split_up(x, split_dim, size)
+    gathered = [pieces[index]]
+    for hop in range(1, size):
+        sent = pieces[index ^ hop]
+        gathered.append(lax.ppermute(sent, axis, [(i, i ^ hop) for i in range(size)]))
+    pieces = jnp.stack(gathered)[index ^ jnp.arange(size)]
+    return joined_along(pieces, concat_dim)
 
 
 def normalize(rows_in):
@@ -46,7 +69,7 @@
         )
         gate_block, up_block = (
             lax.all_to_all(gate_rows, "fs", split_axis=1, concat_axis=0, tiled=True),
-            lax.all_to_all(up_rows, "fs", split_axis=1, concat_axis=0, tiled=True),
+            swapped_with_each(up_rows, "fs", 1, 0),
         )
         total = total + expert_term(
             normed, combine[:, index : index + 1], gate_block, up_block, down_full

time: 773 us -> 801 us (1.036)
  waiting for transfers between devices: 506 us -> 381 us
  local copies, waits for them, and re-layouts: 36.1 us -> 124 us
  starting transfers between devices: 40.6 us -> 110 us
    all_to_all x3 -> x0, waiting for transfers between devices: 172 us -> none  [shards(): lax.all_to_all(up_rows, 'fs', split_axis=1, concat_axis=0, tiled=True)]
    ppermute x0 -> x21, waiting for transfers between devices: none -> 116 us  [swapped_with_each(): lax.ppermute(sent, axis, [(i, i ^ hop) for i in range(size)])]
    ppermute x0 -> x21, starting transfers between devices: none -> 79.8 us  [swapped_with_each(): lax.ppermute(sent, axis, [(i, i ^ hop) for i in range(size)])]
    all_to_all x3, waiting for transfers between devices: 160 us -> 80.7 us  [shards(): lax.all_to_all(gate_rows, 'fs', split_axis=1, concat_axis=0, tiled=True)]
    another operation x0 -> x29, local copies, waits for them, and re-layouts: none -> 41.3 us
    unnamed x10 -> x45, local copies, waits for them, and re-layouts: 16.6 us -> 44.6 us
    all_gather x3, waiting for transfers between devices: 31.4 us -> 47.1 us  [shards(): lax.all_gather(gate_local[index], ('gr', 'tp'), axis=1, tiled=True)]
    gather x0 -> x3, local copies, waits for them, and re-layouts: none -> 14.7 us  [swapped_with_each(): pieces = jnp.stack(gathered)[index ^ jnp.arange(size)]]
  transfers between devices with their start and end apart: 16 -> 34, of which waited for: 9 -> 13; matrix products, arithmetic and copies ran while one was open for 22% -> 30% of each run, Pallas kernels for 0% -> 0%
where the time goes in v1:
time: 801 us; the launch traced here: 794 us
  waiting for transfers between devices  381 us (48%)
  matrix products  125 us (16%)
  local copies, waits for them, and re-layouts  124 us (15%)
  starting transfers between devices  110 us (14%)
  other arithmetic  39.6 us (5%)
  between operations  14.6 us (2%)
    reduce_scatter x1, waiting for transfers between devices, shards(): lax.psum_scatter(total.astype(jnp.bfloat16), 'fs', scatter_dimension=0, t...  119 us
    ppermute x21, waiting for transfers between devices, swapped_with_each(): lax.ppermute(sent, axis, [(i, i ^ hop) for i in range(size)])  116 us
    dot_general x3, matrix products, expert_term(): projected = jnp.dot(hidden, down_weight, preferred_element_type=jnp.float32)  82.6 us
    all_to_all x3, waiting for transfers between devices, shards(): lax.all_to_all(gate_rows, 'fs', split_axis=1, concat_axis=0, tiled=True)  80.7 us
    ppermute x21, starting transfers between devices, swapped_with_each(): lax.ppermute(sent, axis, [(i, i ^ hop) for i in range(size)])  79.8 us
    all_gather x3, waiting for transfers between devices, shards(): lax.all_gather(gate_local[index], ('gr', 'tp'), axis=1, tiled=True)  47.1 us
    unnamed x45, local copies, waits for them, and re-layouts  44.6 us
    dot_general x3, matrix products, expert_term(): gate_act = jnp.dot(normed, gate_weight, preferred_element_type=jnp.float32)  42.7 us
  transfers between devices with their start and end apart: 34, of which 13 were waited for; matrix products, arithmetic and copies ran while one was open for 30% of the time, Pallas kernels for 0%

profile of v1, /device:TPU:0, one launch (start us, length us, event | category | flops | bytes accessed | tf_op | source)
XLA Modules:
  0.0 794.0 jit_solution(15671959436764205879)
XLA Ops:
  7.2 6.1 copy.83
  13.3 6.1 copy.87
  19.4 5.1 multiply_convert_fusion.3
  30.4 2.9 convert_element_type.45
  35.7 24.9 %all-gather.19.cloned.1.call-done = bf16[1,256,7168]{1,2,0:T(8,128)(2,1)} async-done(((bf16[1,256,1792]{1,2,0:T(8,128)(2,1)}), bf16[1,256,7168]{1,2,0:T(8,128)(2,1)}) %all-gather.19.cloned.1.call-update) | async-done | bytes 3670032 | tf_op jit(solution)/shard_map/all_gather | solution.py:66
  60.5 6.2 copy.84
  66.7 5.6 all-to-all-start
  73.3 5.1 fusion
  78.5 15.7 %all-gather.21.cloned.1.call-done = bf16[1,256,7168]{1,2,0:T(8,128)(2,1)} async-done(((bf16[1,256,1792]{1,2,0:T(8,128)(2,1)}), bf16[1,256,7168]{1,2,0:T(8,128)(2,1)}) %all-gather.21.cloned.1.call-update) | async-done | bytes 3670032 | tf_op jit(solution)/shard_map/all_gather | solution.py:66
  94.2 6.2 copy.85
  100.4 54.5 %all-to-all-done = bf16[256,8,896]{2,0,1:T(8,128)(2,1)} async-done(((bf16[256,8,896]{2,0,1:T(8,128)(2,1)}), bf16[256,8,896]{2,0,1:T(8,128)(2,1)}, u32[]{:S(2)}, u32[]{:S(2)}) %all-to-all-start) | async-done | bytes 3670048 | tf_op jit(solution)/shard_map/all_to_all | solution.py:71
  154.8 4.8 all-to-all-start.1
  159.7 3.0 constant_dynamic-slice_fusion.16
  172.2 2.9 collective-permute-start.3
  179.4 13.7 %all-gather.29.cloned.1.call-done = bf16[1,256,7168]{1,2,0:T(8,128)(2,1)} async-done(((bf16[1,256,1792]{1,2,0:T(8,128)(2,1)}), bf16[1,256,7168]{1,2,0:T(8,128)(2,1)}) %all-gather.29.cloned.1.call-update) | async-done | bytes 3670032 | tf_op jit(solution)/shard_map/all_gather | solution.py:67
  193.1 5.2 constant_dynamic-slice_fusion
  201.6 2.0 copy.98
  203.7 2.1 copy.99
  214.0 2.1 copy.105
  220.1 6.6 all-gather.23.cloned.1.call-done
  226.6 6.2 copy.86
  235.3 3.3 collective-permute-start.5
  246.2 46.0 %collective-permute-done.3 = bf16[256,896]{1,0:T(8,128)(2,1)} collective-permute-done((bf16[256,896]{1,0:T(8,128)(2,1)}, bf16[256,896]{1,0:T(8,128)(2,1)}, u32[]{:S(2)}, u32[]{:S(2)}) %collective-permute-start.3) | collective-permute-done | bytes 458784 | tf_op jit(solution)/shard_map/ppermute | solution.py:25
  294.0 8.1 %collective-permute-done.4 = bf16[256,896]{1,0:T(8,128)(2,1)} collective-permute-done((bf16[256,896]{1,0:T(8,128)(2,1)}, bf16[256,896]{1,0:T(8,128)(2,1)}, u32[]{:S(2)}, u32[]{:S(2)}) %collective-permute-start.4) | collective-permute-done | bytes 458784 | tf_op jit(solution)/shard_map/ppermute | solution.py:25
  304.0 7.4 collective-permute-start.10
  312.2 21.2 %collective-permute-start.11 = (bf16[256,896]{1,0:T(8,128)(2,1)}, bf16[256,896]{1,0:T(8,128)(2,1)}, u32[]{:S(2)}, u32[]{:S(2)}) collective-permute-start(bf16[256,896]{1,0:T(8,128)(2,1)} %bitcast.37), channel_id=1, source_target_pairs={{0,10},{2,8},{4,14},{6,12},{8,2},{10,0},{12,6},{14,4},{1,11},{3,9}... | collective-permute-start | bytes 1376264 | tf_op jit(solution)/shard_map/ppermute | solution.py:25
  334.2 5.0 gather_fusion
  339.3 2.3 collective-permute-start.12
  350.1 21.3 %collective-permute-done.10 = bf16[256,896]{1,0:T(8,128)(2,1)} collective-permute-done((bf16[256,896]{1,0:T(8,128)(2,1)}, bf16[256,896]{1,0:T(8,128)(2,1)}, u32[]{:S(2)}, u32[]{:S(2)}) %collective-permute-start.10) | collective-permute-done | bytes 458784 | tf_op jit(solution)/shard_map/ppermute | solution.py:25
  373.2 8.8 %collective-permute-done.11 = bf16[256,896]{1,0:T(8,128)(2,1)} collective-permute-done((bf16[256,896]{1,0:T(8,128)(2,1)}, bf16[256,896]{1,0:T(8,128)(2,1)}, u32[]{:S(2)}, u32[]{:S(2)}) %collective-permute-start.11) | collective-permute-done | bytes 458784 | tf_op jit(solution)/shard_map/ppermute | solution.py:25
  383.8 7.8 collective-permute-start.17
  392.4 21.1 %collective-permute-start.18 = (bf16[256,896]{1,0:T(8,128)(2,1)S(1)}, bf16[256,896]{1,0:T(8,128)(2,1)}, u32[]{:S(2)}, u32[]{:S(2)}) collective-permute-start(bf16[256,896]{1,0:T(8,128)(2,1)S(1)} %bitcast.145), channel_id=1, source_target_pairs={{0,10},{2,8},{4,14},{6,12},{8,2},{10,0},{12,6},{14,4},{1,11},{3,9}... | collective-permute-start | bytes 1376264 | tf_op jit(solution)/shard_map/ppermute | solution.py:25
  414.3 4.8 gather_fusion.1
  428.5 22.5 %collective-permute-done.17 = bf16[256,896]{1,0:T(8,128)(2,1)} collective-permute-done((bf16[256,896]{1,0:T(8,128)(2,1)S(1)}, bf16[256,896]{1,0:T(8,128)(2,1)}, u32[]{:S(2)}, u32[]{:S(2)}) %collective-permute-start.17) | collective-permute-done | bytes 458784 | tf_op jit(solution)/shard_map/ppermute | solution.py:25
  452.9 9.3 %collective-permute-done.18 = bf16[256,896]{1,0:T(8,128)(2,1)} collective-permute-done((bf16[256,896]{1,0:T(8,128)(2,1)S(1)}, bf16[256,896]{1,0:T(8,128)(2,1)}, u32[]{:S(2)}, u32[]{:S(2)}) %collective-permute-start.18) | collective-permute-done | bytes 458784 | tf_op jit(solution)/shard_map/ppermute | solution.py:25
  465.5 4.8 gather_fusion.2
  470.4 18.7 %all-to-all-start.2 = ((bf16[256,8,896]{2,0,1:T(8,128)(2,1)}), bf16[256,8,896]{2,0,1:T(8,128)(2,1)}, u32[]{:S(2)}, u32[]{:S(2)}) async-start(bf16[256,8,896]{2,0,1:T(8,128)(2,1)} %copy.86), calls=%async_computation.2 | async-start | bytes 7340032 | tf_op jit(solution)/shard_map/all_to_all | solution.py:71
  489.7 14.2 %fusion.26 = f32[2048,896]{1,0:T(8,128)} fusion(bf16[2048,896]{1,0:T(8,128)(2,1)} %bitcast.65, bf16[1,2048,2048]{2,1,0:T(8,128)(2,1)} %param.7, f32[2048]{0:T(1024)S(1)} %add_rsqrt_fusion), kind=kOutput, calls=%fused_computation.85 | convolution fusion | flops 7528775680 | bytes 19406848 | tf_op jit(solution)/shard_map/dot_general | solution.py:44
  503.9 14.2 %fusion.22 = f32[2048,896]{1,0:T(8,128)} fusion(bf16[2048,896]{1,0:T(8,128)(2,1)} %bitcast.69, bf16[1,2048,2048]{2,1,0:T(8,128)(2,1)} %param.7, f32[2048]{0:T(1024)S(1)} %add_rsqrt_fusion), kind=kOutput, calls=%fused_computation.84 | convolution fusion | flops 7528775680 | bytes 19406848 | tf_op jit(solution)/shard_map/dot_general | solution.py:44
  518.2 27.0 %fusion.4 = f32[2048,2048]{1,0:T(8,128)} fusion(f32[2048,896]{1,0:T(8,128)} %fusion.26, bf16[2048,896]{1,0:T(8,128)(2,1)} %bitcast.131, bf16[1,896,2048]{2,1,0:T(8,128)(2,1)} %all-gather.31.cloned.1.call-done, bf16[1,2048,2048]{2,1,0:T(8,128)(2,1)} %param.7, f32[2048]{0:T(1024)S(1)} %add_rsqrt_fusion), kind=kOutput, calls=%fused_computation.18 | convolution fusion | flops 15055978496 | bytes 39854080 | tf_op jit(solution)/shard_map/dot_general | solution.py:47
  545.1 26.2 %all-to-all-done.2 = bf16[256,8,896]{2,0,1:T(8,128)(2,1)} async-done(((bf16[256,8,896]{2,0,1:T(8,128)(2,1)}), bf16[256,8,896]{2,0,1:T(8,128)(2,1)}, u32[]{:S(2)}, u32[]{:S(2)}) %all-to-all-start.2) | async-done | bytes 3670048 | tf_op jit(solution)/shard_map/all_to_all | solution.py:71
  571.3 14.2 %fusion.18 = f32[2048,896]{1,0:T(8,128)} fusion(bf16[2048,896]{1,0:T(8,128)(2,1)} %bitcast.73, bf16[1,2048,2048]{2,1,0:T(8,128)(2,1)} %param.7, f32[2048]{0:T(1024)S(1)} %add_rsqrt_fusion), kind=kOutput, calls=%fused_computation.83 | convolution fusion | flops 7528775680 | bytes 19406848 | tf_op jit(solution)/shard_map/dot_general | solution.py:44
  585.6 26.9 %fusion.3 = f32[2048,2048]{1,0:T(8,128)} fusion(f32[2048,896]{1,0:T(8,128)} %fusion.22, bf16[2048,896]{1,0:T(8,128)(2,1)} %bitcast.133, bf16[1,896,2048]{2,1,0:T(8,128)(2,1)} %all-gather.33.cloned.1.call-done, bf16[1,2048,2048]{2,1,0:T(8,128)(2,1)} %param.7, f32[2048]{0:T(1024)S(1)} %add_rsqrt_fusion), kind=kOutput, calls=%fused_computation.17 | convolution fusion | flops 15055978496 | bytes 39854080 | tf_op jit(solution)/shard_map/dot_general | solution.py:47
  612.5 28.7 %add_convert_fusion = bf16[2048,2048]{1,0:T(8,128)(2,1)} fusion(f32[2048,2048]{1,0:T(8,128)} %fusion.3, f32[2048,2048]{1,0:T(8,128)} %fusion.4, f32[2048]{0:T(1024)S(1)} %bitcast.157, f32[2048]{0:T(1024)S(1)} %bitcast.158, f32[2048]{0:T(1024)S(1)} %bitcast.156, f32[2048,896]{1,0:T(8,128)} %fusion.18, bf16[2048,896]{1,0:T(8,128)(2,1)} %bitcast.135, ...), kind=kOutput, calls=%fused_computation.7 | convolution fusion | flops 15081144320 | bytes 65044480 | tf_op jit(solution)/shard_map/dot_general | solution.py:47
  641.2 11.6 %pad_maximum_fusion.2 = bf16[3,896,2048]{2,1,0:T(8,128)(2,1)} fusion(bf16[1,896,2048]{2,1,0:T(8,128)(2,1)} %all-gather.35.cloned.1.call-done, bf16[1,896,2048]{2,1,0:T(8,128)(2,1)} %all-gather.33.cloned.1.call-done, bf16[1,896,2048]{2,1,0:T(8,128)(2,1)} %all-gather.31.cloned.1.call-done), kind=kLoop, calls=%fused_computation.10 | loop fusion | flops 11010048 | bytes 22020096 | tf_op jit(solution)/shard_map/stack | solution.py:82
  652.9 5.0 pad_maximum_fusion.1
  657.9 9.8 %pad_maximum_fusion = bf16[3,2048,896]{2,1,0:T(8,128)(2,1)} fusion(bf16[1,2048,896]{2,1,0:T(8,128)(2,1)} %bitcast.8, bf16[1,2048,896]{2,1,0:T(8,128)(2,1)} %bitcast.5, bf16[1,2048,896]{2,1,0:T(8,128)(2,1)} %bitcast.2), kind=kLoop, calls=%fused_computation.8 | loop fusion | flops 11010048 | bytes 22020096 | tf_op jit(solution)/shard_map/stack | solution.py:80
  667.6 119.3 %reduce-scatter.2.cloned.1.call-done = bf16[256,2048]{1,0:T(8,128)(2,1)} async-done(((bf16[2048,2048]{1,0:T(8,128)(2,1)}), bf16[256,2048]{1,0:T(8,128)(2,1)}) %reduce-scatter.2.cloned.1.call-update) | async-done | bytes 1048592 | tf_op jit(solution)/shard_map/reduce_scatter | solution.py:83
  (132 shorter events, 82.7 us)
Async XLA Ops:
  7.2 53.4 %all-gather.19.cloned.1.call-start = ((), (), s32[]{:S(2)}) async-start(), calls=%async_computation.5 | async-start | bytes 4587520 | tf_op jit(solution)/shard_map/all_gather | solution.py:66
  13.3 6.1 copy-start.10
  26.2 68.0 %all-gather.21.cloned.1.call-start = ((), (), s32[]{:S(2)}) async-start(), calls=%async_computation.6 | async-start | bytes 4587520 | tf_op jit(solution)/shard_map/all_gather | solution.py:66
  26.9 132.7 %all-gather.25.cloned.1.call-start = ((), (), s32[]{:S(2)}) async-start(), calls=%async_computation.8 | async-start | bytes 4587520 | tf_op jit(solution)/shard_map/all_gather | solution.py:67
  28.6 150.8 %all-gather.27.cloned.1.call-start = ((), (), s32[]{:S(2)}) async-start(), calls=%async_computation.9 | async-start | bytes 4587520 | tf_op jit(solution)/shard_map/all_gather | solution.py:67
  29.2 164.0 %all-gather.29.cloned.1.call-start = ((), (), s32[]{:S(2)}) async-start(), calls=%async_computation.10 | async-start | bytes 4587520 | tf_op jit(solution)/shard_map/all_gather | solution.py:67
  29.8 196.9 %all-gather.23.cloned.1.call-start = ((), (), s32[]{:S(2)}) async-start(), calls=%async_computation.7 | async-start | bytes 4587520 | tf_op jit(solution)/shard_map/all_gather | solution.py:66
  30.3 487.8 %all-gather.31.cloned.1.call-start = ((), (), s32[]{:S(2)}) async-start(), calls=%async_computation.11 | async-start | bytes 4587520 | tf_op jit(solution)/shard_map/all_gather | solution.py:68
  34.9 550.6 %all-gather.33.cloned.1.call-start = ((), (), s32[]{:S(2)}) async-start(), calls=%async_computation.12 | async-start | bytes 4587520 | tf_op jit(solution)/shard_map/all_gather | solution.py:68
  66.7 6.4 copy-start.8
  66.7 6.5 copy-start.9
  66.7 88.1 %all-to-all-start = ((bf16[256,8,896]{2,0,1:T(8,128)(2,1)}), bf16[256,8,896]{2,0,1:T(8,128)(2,1)}, u32[]{:S(2)}, u32[]{:S(2)}) async-start(bf16[256,8,896]{2,0,1:T(8,128)(2,1)} %copy.84), calls=%async_computation | async-start | bytes 7340032 | tf_op jit(solution)/shard_map/all_to_all | solution.py:71
  72.4 540.1 %all-gather.35.cloned.1.call-start = ((), (), s32[]{:S(2)}) async-start(), calls=%async_computation.13 | async-start | bytes 4587520 | tf_op jit(solution)/shard_map/all_gather | solution.py:68
  154.8 315.5 %all-to-all-start.1 = ((bf16[256,8,896]{2,0,1:T(8,128)(2,1)}), bf16[256,8,896]{2,0,1:T(8,128)(2,1)}, u32[]{:S(2)}, u32[]{:S(2)}) async-start(bf16[256,8,896]{2,0,1:T(8,128)(2,1)} %copy.85), calls=%async_computation.1 | async-start | bytes 7340032 | tf_op jit(solution)/shard_map/all_to_all | solution.py:71
  165.7 69.6 %collective-permute-start = (bf16[256,896]{1,0:T(8,128)(2,1)}, bf16[256,896]{1,0:T(8,128)(2,1)}, u32[]{:S(2)}, u32[]{:S(2)}) collective-permute-start(bf16[256,896]{1,0:T(8,128)(2,1)} %bitcast.154), channel_id=1, source_target_pairs={{0,2},{2,0},{4,6},{6,4},{8,10},{10,8},{12,14},{14,12},{1,3},{3,1},... | collective-permute-start | bytes 1376264 | tf_op jit(solution)/shard_map/ppermute | solution.py:25
  168.6 71.8 %collective-permute-start.1 = (bf16[256,896]{1,0:T(8,128)(2,1)}, bf16[256,896]{1,0:T(8,128)(2,1)}, u32[]{:S(2)}, u32[]{:S(2)}) collective-permute-start(bf16[256,896]{1,0:T(8,128)(2,1)} %bitcast.13), channel_id=1, source_target_pairs={{0,4},{2,6},{4,0},{6,2},{8,12},{10,14},{12,8},{14,10},{1,5},{3,7},... | collective-permute-start | bytes 1376264 | tf_op jit(solution)/shard_map/ppermute | solution.py:25
  171.1 72.6 %collective-permute-start.2 = (bf16[256,896]{1,0:T(8,128)(2,1)}, bf16[256,896]{1,0:T(8,128)(2,1)}, u32[]{:S(2)}, u32[]{:S(2)}) collective-permute-start(bf16[256,896]{1,0:T(8,128)(2,1)} %bitcast.15), channel_id=1, source_target_pairs={{0,6},{2,4},{4,2},{6,0},{8,14},{10,12},{12,10},{14,8},{1,7},{3,5},... | collective-permute-start | bytes 1376264 | tf_op jit(solution)/shard_map/ppermute | solution.py:25
  172.2 120.0 %collective-permute-start.3 = (bf16[256,896]{1,0:T(8,128)(2,1)}, bf16[256,896]{1,0:T(8,128)(2,1)}, u32[]{:S(2)}, u32[]{:S(2)}) collective-permute-start(bf16[256,896]{1,0:T(8,128)(2,1)} %bitcast.17), channel_id=1, source_target_pairs={{0,8},{2,10},{4,12},{6,14},{8,0},{10,2},{12,4},{14,6},{1,9},{3,11}... | collective-permute-start | bytes 1376264 | tf_op jit(solution)/shard_map/ppermute | solution.py:25
  176.0 126.1 %collective-permute-start.4 = (bf16[256,896]{1,0:T(8,128)(2,1)}, bf16[256,896]{1,0:T(8,128)(2,1)}, u32[]{:S(2)}, u32[]{:S(2)}) collective-permute-start(bf16[256,896]{1,0:T(8,128)(2,1)} %bitcast.19), channel_id=1, source_target_pairs={{0,10},{2,8},{4,14},{6,12},{8,2},{10,0},{12,6},{14,4},{1,11},{3,9}... | collective-permute-start | bytes 1376264 | tf_op jit(solution)/shard_map/ppermute | solution.py:25
  226.6 6.3 copy-start.3
  232.9 7.6 copy-start.7
  235.3 68.7 %collective-permute-start.5 = (bf16[256,896]{1,0:T(8,128)(2,1)}, bf16[256,896]{1,0:T(8,128)(2,1)S(1)}, u32[]{:S(2)}, u32[]{:S(2)}) collective-permute-start(bf16[256,896]{1,0:T(8,128)(2,1)} %bitcast.153), channel_id=1, source_target_pairs={{0,12},{2,14},{4,8},{6,10},{8,4},{10,6},{12,0},{14,2},{1,13},{3,15... | collective-permute-start | bytes 1376264 | tf_op jit(solution)/shard_map/ppermute | solution.py:25
  240.5 71.7 %collective-permute-start.6 = (bf16[256,896]{1,0:T(8,128)(2,1)S(1)}, bf16[256,896]{1,0:T(8,128)(2,1)S(1)}, u32[]{:S(2)}, u32[]{:S(2)}) collective-permute-start(bf16[256,896]{1,0:T(8,128)(2,1)S(1)} %bitcast.152), channel_id=1, source_target_pairs={{0,14},{2,12},{4,10},{6,8},{8,6},{10,4},{12,2},{14,0},{1,15},{3,13... | collective-permute-start | bytes 1376264 | tf_op jit(solution)/shard_map/ppermute | solution.py:25
  243.8 95.5 %collective-permute-start.7 = (bf16[256,896]{1,0:T(8,128)(2,1)}, bf16[256,896]{1,0:T(8,128)(2,1)}, u32[]{:S(2)}, u32[]{:S(2)}) collective-permute-start(bf16[256,896]{1,0:T(8,128)(2,1)} %bitcast.29), channel_id=1, source_target_pairs={{0,2},{2,0},{4,6},{6,4},{8,10},{10,8},{12,14},{14,12},{1,3},{3,1},... | collective-permute-start | bytes 1376264 | tf_op jit(solution)/shard_map/ppermute | solution.py:25
  292.2 51.2 %collective-permute-start.8 = (bf16[256,896]{1,0:T(8,128)(2,1)}, bf16[256,896]{1,0:T(8,128)(2,1)}, u32[]{:S(2)}, u32[]{:S(2)}) collective-permute-start(bf16[256,896]{1,0:T(8,128)(2,1)} %bitcast.31), channel_id=1, source_target_pairs={{0,4},{2,6},{4,0},{6,2},{8,12},{10,14},{12,8},{14,10},{1,5},{3,7},... | collective-permute-start | bytes 1376264 | tf_op jit(solution)/shard_map/ppermute | solution.py:25
  302.2 44.7 %collective-permute-start.9 = (bf16[256,896]{1,0:T(8,128)(2,1)}, bf16[256,896]{1,0:T(8,128)(2,1)}, u32[]{:S(2)}, u32[]{:S(2)}) collective-permute-start(bf16[256,896]{1,0:T(8,128)(2,1)} %bitcast.33), channel_id=1, source_target_pairs={{0,6},{2,4},{4,2},{6,0},{8,14},{10,12},{12,10},{14,8},{1,7},{3,5},... | collective-permute-start | bytes 1376264 | tf_op jit(solution)/shard_map/ppermute | solution.py:25
  304.0 67.4 %collective-permute-start.10 = (bf16[256,896]{1,0:T(8,128)(2,1)}, bf16[256,896]{1,0:T(8,128)(2,1)}, u32[]{:S(2)}, u32[]{:S(2)}) collective-permute-start(bf16[256,896]{1,0:T(8,128)(2,1)} %bitcast.35), channel_id=1, source_target_pairs={{0,8},{2,10},{4,12},{6,14},{8,0},{10,2},{12,4},{14,6},{1,9},{3,11}... | collective-permute-start | bytes 1376264 | tf_op jit(solution)/shard_map/ppermute | solution.py:25
  312.2 69.8 %collective-permute-start.11 = (bf16[256,896]{1,0:T(8,128)(2,1)}, bf16[256,896]{1,0:T(8,128)(2,1)}, u32[]{:S(2)}, u32[]{:S(2)}) collective-permute-start(bf16[256,896]{1,0:T(8,128)(2,1)} %bitcast.37), channel_id=1, source_target_pairs={{0,10},{2,8},{4,14},{6,12},{8,2},{10,0},{12,6},{14,4},{1,11},{3,9}... | collective-permute-start | bytes 1376264 | tf_op jit(solution)/shard_map/ppermute | solution.py:25
  334.2 12.6 %copy-start.6 = (bf16[256,1,896]{2,0,1:T(8,128)(2,1)S(1)}, bf16[256,1,896]{2,0,1:T(8,128)(2,1)}, u32[]{:S(2)}) copy-start(bf16[256,1,896]{2,0,1:T(8,128)(2,1)} %copy.105) | copy-start | bytes 1376260
  334.2 37.1 %copy-start.5 = (bf16[256,1,896]{2,0,1:T(8,128)(2,1)S(1)}, bf16[256,1,896]{2,0,1:T(8,128)(2,1)}, u32[]{:S(2)}) copy-start(bf16[256,1,896]{2,0,1:T(8,128)(2,1)} %copy.106) | copy-start | bytes 1376260
  339.3 42.7 %copy-start.4 = (bf16[256,1,896]{2,0,1:T(8,128)(2,1)S(1)}, bf16[256,1,896]{2,0,1:T(8,128)(2,1)}, u32[]{:S(2)}) copy-start(bf16[256,1,896]{2,0,1:T(8,128)(2,1)} %copy.107) | copy-start | bytes 1376260
  339.3 44.5 %collective-permute-start.12 = (bf16[256,896]{1,0:T(8,128)(2,1)}, bf16[256,896]{1,0:T(8,128)(2,1)S(1)}, u32[]{:S(2)}, u32[]{:S(2)}) collective-permute-start(bf16[256,896]{1,0:T(8,128)(2,1)} %bitcast.151), channel_id=1, source_target_pairs={{0,12},{2,14},{4,8},{6,10},{8,4},{10,6},{12,0},{14,2},{1,13},{3,15... | collective-permute-start | bytes 1376264 | tf_op jit(solution)/shard_map/ppermute | solution.py:25
  343.3 49.0 %collective-permute-start.13 = (bf16[256,896]{1,0:T(8,128)(2,1)}, bf16[256,896]{1,0:T(8,128)(2,1)S(1)}, u32[]{:S(2)}, u32[]{:S(2)}) collective-permute-start(bf16[256,896]{1,0:T(8,128)(2,1)} %bitcast.150), channel_id=1, source_target_pairs={{0,14},{2,12},{4,10},{6,8},{8,6},{10,4},{12,2},{14,0},{1,15},{3,13... | collective-permute-start | bytes 1376264 | tf_op jit(solution)/shard_map/ppermute | solution.py:25
  346.9 72.3 %collective-permute-start.14 = (bf16[256,896]{1,0:T(8,128)(2,1)S(1)}, bf16[256,896]{1,0:T(8,128)(2,1)}, u32[]{:S(2)}, u32[]{:S(2)}) collective-permute-start(bf16[256,896]{1,0:T(8,128)(2,1)S(1)} %bitcast.149), channel_id=1, source_target_pairs={{0,2},{2,0},{4,6},{6,4},{8,10},{10,8},{12,14},{14,12},{1,3},{3,1},... | collective-permute-start | bytes 1376264 | tf_op jit(solution)/shard_map/ppermute | solution.py:25
  371.4 51.6 %collective-permute-start.15 = (bf16[256,896]{1,0:T(8,128)(2,1)S(1)}, bf16[256,896]{1,0:T(8,128)(2,1)}, u32[]{:S(2)}, u32[]{:S(2)}) collective-permute-start(bf16[256,896]{1,0:T(8,128)(2,1)S(1)} %bitcast.148), channel_id=1, source_target_pairs={{0,4},{2,6},{4,0},{6,2},{8,12},{10,14},{12,8},{14,10},{1,5},{3,7},... | collective-permute-start | bytes 1376264 | tf_op jit(solution)/shard_map/ppermute | solution.py:25
  382.0 44.7 %collective-permute-start.16 = (bf16[256,896]{1,0:T(8,128)(2,1)S(1)}, bf16[256,896]{1,0:T(8,128)(2,1)}, u32[]{:S(2)}, u32[]{:S(2)}) collective-permute-start(bf16[256,896]{1,0:T(8,128)(2,1)S(1)} %bitcast.147), channel_id=1, source_target_pairs={{0,6},{2,4},{4,2},{6,0},{8,14},{10,12},{12,10},{14,8},{1,7},{3,5},... | collective-permute-start | bytes 1376264 | tf_op jit(solution)/shard_map/ppermute | solution.py:25
  383.8 67.2 %collective-permute-start.17 = (bf16[256,896]{1,0:T(8,128)(2,1)S(1)}, bf16[256,896]{1,0:T(8,128)(2,1)}, u32[]{:S(2)}, u32[]{:S(2)}) collective-permute-start(bf16[256,896]{1,0:T(8,128)(2,1)S(1)} %bitcast.146), channel_id=1, source_target_pairs={{0,8},{2,10},{4,12},{6,14},{8,0},{10,2},{12,4},{14,6},{1,9},{3,11}... | collective-permute-start | bytes 1376264 | tf_op jit(solution)/shard_map/ppermute | solution.py:25
  392.4 69.7 %collective-permute-start.18 = (bf16[256,896]{1,0:T(8,128)(2,1)S(1)}, bf16[256,896]{1,0:T(8,128)(2,1)}, u32[]{:S(2)}, u32[]{:S(2)}) collective-permute-start(bf16[256,896]{1,0:T(8,128)(2,1)S(1)} %bitcast.145), channel_id=1, source_target_pairs={{0,10},{2,8},{4,14},{6,12},{8,2},{10,0},{12,6},{14,4},{1,11},{3,9}... | collective-permute-start | bytes 1376264 | tf_op jit(solution)/shard_map/ppermute | solution.py:25
  419.1 44.8 %collective-permute-start.19 = (bf16[256,896]{1,0:T(8,128)(2,1)S(1)}, bf16[256,896]{1,0:T(8,128)(2,1)S(1)}, u32[]{:S(2)}, u32[]{:S(2)}) collective-permute-start(bf16[256,896]{1,0:T(8,128)(2,1)S(1)} %bitcast.144), channel_id=1, source_target_pairs={{0,12},{2,14},{4,8},{6,10},{8,4},{10,6},{12,0},{14,2},{1,13},{3,15... | collective-permute-start | bytes 1376264 | tf_op jit(solution)/shard_map/ppermute | solution.py:25
  422.9 41.8 %collective-permute-start.20 = (bf16[256,896]{1,0:T(8,128)(2,1)S(1)}, bf16[256,896]{1,0:T(8,128)(2,1)S(1)}, u32[]{:S(2)}, u32[]{:S(2)}) collective-permute-start(bf16[256,896]{1,0:T(8,128)(2,1)S(1)} %bitcast.143), channel_id=1, source_target_pairs={{0,14},{2,12},{4,10},{6,8},{8,6},{10,4},{12,2},{14,0},{1,15},{3,13... | collective-permute-start | bytes 1376264 | tf_op jit(solution)/shard_map/ppermute | solution.py:25
  470.4 101.0 %all-to-all-start.2 = ((bf16[256,8,896]{2,0,1:T(8,128)(2,1)}), bf16[256,8,896]{2,0,1:T(8,128)(2,1)}, u32[]{:S(2)}, u32[]{:S(2)}) async-start(bf16[256,8,896]{2,0,1:T(8,128)(2,1)} %copy.86), calls=%async_computation.2 | async-start | bytes 7340032 | tf_op jit(solution)/shard_map/all_to_all | solution.py:71
  489.1 297.8 %reduce-scatter.2.cloned.1.call-start = ((), (), s32[]{:S(2)}) async-start(), calls=%async_computation.4 | async-start | bytes 9437184 | tf_op jit(solution)/shard_map/reduce_scatter | solution.py:83
  641.2 11.6 %copy-start = (bf16[8,256,896]{2,1,0:T(8,128)(2,1)S(1)}, bf16[8,256,896]{2,1,0:T(8,128)(2,1)}, u32[]{:S(2)}) copy-start(bf16[8,256,896]{2,1,0:T(8,128)(2,1)} %gather_fusion) | copy-start | bytes 11010052
  641.2 11.6 %copy-start.1 = (bf16[8,256,896]{2,1,0:T(8,128)(2,1)S(1)}, bf16[8,256,896]{2,1,0:T(8,128)(2,1)}, u32[]{:S(2)}) copy-start(bf16[8,256,896]{2,1,0:T(8,128)(2,1)} %gather_fusion.1) | copy-start | bytes 11010052
  641.2 11.6 %copy-start.2 = (bf16[8,256,896]{2,1,0:T(8,128)(2,1)S(1)}, bf16[8,256,896]{2,1,0:T(8,128)(2,1)}, u32[]{:S(2)}) copy-start(bf16[8,256,896]{2,1,0:T(8,128)(2,1)} %gather_fusion.2) | copy-start | bytes 11010052
Sparse Core Ops, SparseCore 0:
  26.3 34.1 all-gather.18
  62.7 31.4 all-gather.20
  95.8 31.4 all-gather.24
  128.7 31.4 all-gather.26
  161.6 31.4 all-gather.28
  195.1 31.4 all-gather.22
  228.2 31.4 all-gather.30
  261.3 31.4 all-gather.32
  294.4 31.4 all-gather.34
  641.3 145.5 reduce-scatter.1
